TPU v7x, 32 devices: a whole 2x2x4 slice. The times are simulated.
32 devices in a mesh: kv: 8 (over z, x), tp: 4 (over y, core).
Axes of the slice: x: 2, y: 2, z: 4, core: 2. Of those that a mesh axis runs over, the one named last changes fastest.
Arguments:
- inputs: bfloat16 [4, 2048, 2048], P(None, 'kv'), may hold values from -40 to 40
- query_weight: bfloat16 [2048, 2048], P(None, 'tp'), may hold values from -0.125 to 0.125
- key_weight: bfloat16 [2048, 1024], P(None, 'tp'), may hold values from -0.125 to 0.125
- value_weight: bfloat16 [2048, 1024], P(None, 'tp'), may hold values from -0.125 to 0.125
- out_weight: bfloat16 [2048, 2048], P('tp'), may hold values from -1 to 1
- chosen: int32 [4, 32, 32], P(None, 'kv'), may hold values from 0 to 31, as said below
- lengths: int32 [4], replicated, may hold values from 1 to 2048, 3072 in all
Outputs:
- mixed: bfloat16 [4, 2048, 2048], P(None, 'kv', 'tp')
Inputs may be any that keep to these rules, and one draw needn't show every extreme that they name: chosen[b, q, 0] = q; every entry names a block of the same sequence at or before q; entries may repeat. Over the query blocks of positions k * 256 to (k+1) * 256 - 1 of all sequences, the named blocks that lie in another span of 256 positions number at most 3 distinct blocks for each other span, and 3 is reached.
All inputs are finite; a program needn't handle non-finite values.
Results may differ from a plain program's by a relative error of at most 0.014.
The roundings to bfloat16 on the way count: a program that leaves them out, or rounds other values in their place, can miss the bound.
Values may be sent and summed in bfloat16 or wider, within the bound.
A program may use at most 128 MiB of HBM per device.

v0:
```python
import jax
import jax.numpy as jnp
from jax import lax
from jax.sharding import PartitionSpec as P

HD = 128
KB = 64
TOPK = 32
CAP = 3


def unique_slots(chosen_rows):
    order = jnp.arange(TOPK, dtype=jnp.int32)
    repeated = jnp.any(
        (chosen_rows[..., :, None] == chosen_rows[..., None, :])
        & (order[:, None] > order[None, :]),
        axis=-1,
    )
    return jnp.repeat(jnp.logical_not(repeated), KB, axis=-1)


def attend(queries, key_sets, value_sets, key_pos, unique_key, query_pos, live_length, scaling):
    scores = (
        jnp.einsum("nqkgd,npkd->nkgqp", queries, key_sets, preferred_element_type=jnp.float32)
        * scaling
    )
    allowed = (
        (key_pos[:, None, :] <= query_pos[:, :, None])
        & (key_pos[:, None, :] < live_length)
        & unique_key[:, None, :]
    )
    allowed = allowed | (key_pos[:, None, :] == query_pos[:, :, None])
    scores = jnp.where(allowed[:, None, None], scores, -jnp.inf)
    highest = jnp.max(scores, axis=-1, keepdims=True)
    raised = jnp.exp(scores - highest)
    weights = (raised / jnp.sum(raised, axis=-1, keepdims=True)).astype(jnp.bfloat16)
    combined = jnp.einsum(
        "nkgqp,npkd->nqkgd", weights, value_sets, preferred_element_type=jnp.float32
    )
    living = (query_pos < live_length)[:, :, None, None, None]
    return jnp.where(living, combined, 0.0).astype(jnp.bfloat16)


def shards(inputs, query_weight, key_weight, value_weight, out_weight, chosen, lengths):
    batch_size, positions, model_width = inputs.shape
    kv_local = key_weight.shape[1] // HD
    heads_local = query_weight.shape[1] // HD
    per_group = heads_local // kv_local
    per_dev = positions // KB
    owned = batch_size * per_dev
    device = lax.axis_index("kv")
    devices = lax.axis_size("kv")
    flat_rows = inputs.reshape(batch_size * positions, model_width)
    queries = jnp.dot(flat_rows, query_weight, preferred_element_type=jnp.float32).astype(
        jnp.bfloat16
    )
    queries = queries.reshape(batch_size, per_dev, KB, kv_local, per_group, HD)
    key_rows = jnp.dot(flat_rows, key_weight, preferred_element_type=jnp.float32).astype(
        jnp.bfloat16
    )
    key_rows = key_rows.reshape(owned, KB, kv_local * HD)
    value_rows = jnp.dot(flat_rows, value_weight, preferred_element_type=jnp.float32).astype(
        jnp.bfloat16
    )
    value_rows = value_rows.reshape(owned, KB, kv_local * HD)
    seq_base = jnp.arange(batch_size, dtype=jnp.int32)[:, None, None]
    owners = chosen // per_dev
    local_block = seq_base * per_dev + chosen % per_dev
    one_hot = (owners * owned + local_block).reshape(-1)[:, None] == jnp.arange(
        devices * owned, dtype=jnp.int32
    )[None, :]
    needed = jnp.any(one_hot, axis=0).reshape(devices, owned) & (
        jnp.arange(devices, dtype=jnp.int32)[:, None] != device
    )
    slots = jnp.cumsum(needed.astype(jnp.int32), axis=1) - 1
    matches = needed[:, :, None] & (
        slots[:, :, None] == jnp.arange(CAP, dtype=jnp.int32)[None, None, :]
    )
    requests = jnp.sum(
        jnp.where(matches, jnp.arange(owned, dtype=jnp.int32)[None, :, None], 0), axis=1
    )
    asked = lax.all_to_all(requests, "kv", split_axis=0, concat_axis=0, tiled=True)
    got_keys, got_values = (
        lax.all_to_all(key_rows[asked], "kv", split_axis=0, concat_axis=0, tiled=True),
        lax.all_to_all(value_rows[asked], "kv", split_axis=0, concat_axis=0, tiled=True),
    )
    key_table = jnp.concatenate(
        [key_rows, got_keys.reshape(devices * CAP, KB, kv_local * HD)], axis=0
    )
    value_table = jnp.concatenate(
        [value_rows, got_values.reshape(devices * CAP, KB, kv_local * HD)], axis=0
    )
    slot_of = jnp.sum(jnp.where(one_hot, slots.reshape(-1)[None, :], 0), axis=1).reshape(
        chosen.shape
    )
    table_rows = jnp.where(owners == device, local_block, owned + owners * CAP + slot_of)
    offsets = jnp.arange(KB, dtype=jnp.int32)
    query_pos = (device * per_dev + jnp.arange(per_dev, dtype=jnp.int32))[:, None] * KB + offsets[
        None, :
    ]
    key_pos = (chosen[..., None] * KB + offsets).reshape(batch_size, per_dev, TOPK * KB)
    unique_key = unique_slots(chosen)
    scaling = HD ** (-0.5)

    def one_seq(seq_inputs):
        seq_queries, seq_rows, seq_key_pos, seq_unique, live_length = seq_inputs
        key_sets = key_table[seq_rows].reshape(per_dev, TOPK * KB, kv_local, HD)
        value_sets = value_table[seq_rows].reshape(per_dev, TOPK * KB, kv_local, HD)
        return attend(
            seq_queries,
            key_sets,
            value_sets,
            seq_key_pos,
            seq_unique,
            query_pos,
            live_length,
            scaling,
        )

    attended = lax.map(one_seq, (queries, table_rows, key_pos, unique_key, lengths))
    attended = attended.reshape(batch_size * positions, heads_local * HD)
    partial_value = jnp.dot(attended, out_weight, preferred_element_type=jnp.float32).astype(
        jnp.bfloat16
    )
    partial_value = (
        lax.optimization_barrier(partial_value)
        .astype(jnp.float32)
        .reshape(batch_size, positions, model_width)
    )
    return lax.psum_scatter(
        partial_value.astype(jnp.bfloat16), "tp", scatter_dimension=2, tiled=True
    )


def solution(mesh):
    placed = (
        P(None, "kv", None),
        P(None, "tp"),
        P(None, "tp"),
        P(None, "tp"),
        P("tp", None),
        P(None, "kv", None),
        P(),
    )
    return jax.shard_map(
        shards, mesh=mesh, in_specs=placed, out_specs=P(None, "kv", "tp"), check_vma=False
    )
```

profile of v0, /device:TPU:0, one launch (start us, length us, event | category | flops | bytes accessed | tf_op | source)
XLA Modules:
  0.0 305.6 jit_solution(2691484994486179288)
XLA Ops:
  8.9 7.3 %all-to-all-start = ((s32[8,1,3]{2,1,0:T(1,128)}), s32[8,1,3]{2,1,0:T(1,128)S(1)}, u32[]{:S(2)}, u32[]{:S(2)}) async-start(s32[8,1,3]{2,1,0:T(1,128)} %copy.26), calls=%async_computation | async-start | bytes 8192 | tf_op jit(solution)/shard_map/all_to_all | solution.py:82
  16.2 3.7 %convolution_convert_fusion.3 = bf16[1024,256]{1,0:T(8,128)(2,1)S(1)} fusion(bf16[1024,2048]{1,0:T(8,128)(2,1)} %bitcast.80, bf16[2048,256]{1,0:T(8,128)(2,1)} %param.12), kind=kOutput, calls=%fused_computation.38 | convolution fusion | flops 1074003968 | bytes 5767168 | tf_op jit(solution)/shard_map/dot_general | solution.py:62
  24.4 4.2 %all-to-all-start.1 = ((bf16[8,3,64,256]{3,2,1,0:T(8,128)(2,1)}), bf16[8,3,64,256]{3,2,1,0:T(8,128)(2,1)}, u32[]{:S(2)}, u32[]{:S(2)}) async-start(bf16[8,3,64,256]{3,2,1,0:T(8,128)(2,1)} %bitcast.4), calls=%async_computation.1 | async-start | bytes 1572864 | tf_op jit(solution)/shard_map/all_to_all | solution.py:85
  28.6 3.7 %convolution_convert_fusion.2 = bf16[1024,256]{1,0:T(8,128)(2,1)S(1)} fusion(bf16[1024,2048]{1,0:T(8,128)(2,1)} %bitcast.81, bf16[2048,256]{1,0:T(8,128)(2,1)} %param.11), kind=kOutput, calls=%fused_computation.37 | convolution fusion | flops 1074003968 | bytes 5767168 | tf_op jit(solution)/shard_map/dot_general | solution.py:58
  33.8 13.8 %all-to-all-done.1 = bf16[8,3,64,256]{3,2,1,0:T(8,128)(2,1)} async-done(((bf16[8,3,64,256]{3,2,1,0:T(8,128)(2,1)}), bf16[8,3,64,256]{3,2,1,0:T(8,128)(2,1)}, u32[]{:S(2)}, u32[]{:S(2)}) %all-to-all-start.1) | async-done | bytes 786464 | tf_op jit(solution)/shard_map/all_to_all | solution.py:85
  47.7 4.2 %all-to-all-start.2 = ((bf16[8,3,64,256]{3,2,1,0:T(8,128)(2,1)}), bf16[8,3,64,256]{3,2,1,0:T(8,128)(2,1)}, u32[]{:S(2)}, u32[]{:S(2)}) async-start(bf16[8,3,64,256]{3,2,1,0:T(8,128)(2,1)} %bitcast.78), calls=%async_computation.2 | async-start | bytes 1572864 | tf_op jit(solution)/shard_map/all_to_all | solution.py:84
  52.1 6.2 %convolution_convert_fusion.1 = bf16[1024,512]{1,0:T(8,128)(2,1)} fusion(bf16[1024,2048]{1,0:T(8,128)(2,1)} %bitcast.82, bf16[2048,512]{1,0:T(8,128)(2,1)} %param.10), kind=kOutput, calls=%fused_computation.34 | convolution fusion | flops 2148007936 | bytes 7340032 | tf_op jit(solution)/shard_map/dot_general | solution.py:54
  64.8 6.6 %all-to-all-done.2 = bf16[8,3,64,256]{3,2,1,0:T(8,128)(2,1)} async-done(((bf16[8,3,64,256]{3,2,1,0:T(8,128)(2,1)}), bf16[8,3,64,256]{3,2,1,0:T(8,128)(2,1)}, u32[]{:S(2)}, u32[]{:S(2)}) %all-to-all-start.2) | async-done | bytes 786464 | tf_op jit(solution)/shard_map/all_to_all | solution.py:84
  73.8 175.5 %while.11 = (s32[]{:T(128)}, bf16[4,4,64,2,2,128]{5,4,3,2,1,0:T(2,128)(2,1)}, s32[4]{0:T(128)}, s32[4,4,32]{2,1,0:T(4,128)S(1)}, bf16[40,64,256]{2,1,0:T(8,128)(...) while((s32[]{:T(128)}, ...), condition=%wide.region_8.9_spmd.clone, body=%wide.region_5.8_spmd.clone.sunk | while | flops 1093415040 | bytes 80374576 | solution.py:120
  78.2 4.1 %gather_fusion = bf16[128,64,256]{2,1,0:T(8,128)(2,1)} fusion(bf16[40,64,256]{2,1,0:T(8,128)(2,1)} %get-tuple-element.247, s32[1024]{0:T(1024)S(1)} %pad_clamp_fusion.3), kind=kCustom, calls=%fused_computation.1.clone.clone.1 | custom fusion | bytes 8389120 | tf_op jit(solution)/shard_map/while/body/eval_jaxpr/gather | solution.py:107
  82.3 6.9 %reshape.252 = bf16[4,2048,2,128]{3,2,1,0:T(2,128)(2,1)} reshape(bf16[128,64,256]{2,1,0:T(8,128)(2,1)} %gather_fusion) | data formatting | bytes 8388608 | tf_op jit(solution)/shard_map/while/body/eval_jaxpr/reshape | solution.py:107
  90.3 3.5 %fusion.43 = f32[4,2,2048,64,2]{2,3,4,1,0:T(8,128)S(1)} fusion(bf16[4,2048,2,128,1]{3,2,1,0,4:T(2,128)(2,1)} %bitcast.71, bf16[1,4,64,2,2,128]{5,4,3,2,1,0:T(2,128)(2,1)S(1)} %constant_dynamic-slice_fusion.2), kind=kOutput, calls=%fused_computation.10.clone.1 | convolution fusion | flops 536870912 | bytes 12845056 | tf_op jit(solution)/shard_map/while/body/eval_jaxpr/nqkgd,npkd->nkgqp/dot_general | solution.py:24
  93.9 5.9 %fusion.44 = (f32[4,2,2,64]{3,2,1,0:T(2,128)}, f32[4,2,2,64,2048]{4,3,2,1,0:T(8,128)}) fusion(f32[4,2,2048,64,2]{2,3,4,1,0:T(8,128)S(1)} %fusion.43, pred[4,64,2048]{2,1,0:T(8,128)(4,1)S(1)} %copy-done.1), kind=kOutput, calls=%fused_computation.68.clone.1 | output fusion | flops 12584959 | bytes 17305600 | tf_op jit(solution)/shard_map/while/body/eval_jaxpr/sub | solution.py:35
  103.9 6.9 %reshape.253 = bf16[4,2048,2,128]{3,2,1,0:T(2,128)(2,1)} reshape(bf16[128,64,256]{2,1,0:T(8,128)(2,1)} %gather_fusion.1) | data formatting | bytes 8388608 | tf_op jit(solution)/shard_map/while/body/eval_jaxpr/reshape | solution.py:108
  110.8 5.9 %fusion.45 = bf16[1,4,64,2,2,128]{5,2,4,3,1,0:T(8,128)(2,1)S(1)} fusion(f32[4,2,2,64,2048]{4,3,2,1,0:T(8,128)} %get-tuple-element.216, f32[4,2,2,64]{3,2,1,0:T(2,128)} %get-tuple-element.217, bf16[4,2048,2,128,1]{3,2,1,0,4:T(2,128)(2,1)} %bitcast.72, pred[4,64]{1,0:T(4,128)(4,1)S(1)} %broadcast_compare_fusion.6), kind=kOutput, calls=%fused_computation.20.clone.1 | convolution fusion | flops 541327360 | bytes 12849408 | tf_op jit(solution)/shard_map/while/body/eval_jaxpr/nkgqp,npkd->nqkgd/dot_general | solution.py:37
  122.1 4.1 %gather_fusion = bf16[128,64,256]{2,1,0:T(8,128)(2,1)} fusion(bf16[40,64,256]{2,1,0:T(8,128)(2,1)} %get-tuple-element.247, s32[1024]{0:T(1024)S(1)} %pad_clamp_fusion.3), kind=kCustom, calls=%fused_computation.1.clone.clone.1 | custom fusion | bytes 8389120 | tf_op jit(solution)/shard_map/while/body/eval_jaxpr/gather | solution.py:107
  126.2 6.9 %reshape.252 = bf16[4,2048,2,128]{3,2,1,0:T(2,128)(2,1)} reshape(bf16[128,64,256]{2,1,0:T(8,128)(2,1)} %gather_fusion) | data formatting | bytes 8388608 | tf_op jit(solution)/shard_map/while/body/eval_jaxpr/reshape | solution.py:107
  137.7 5.9 %fusion.44 = (f32[4,2,2,64]{3,2,1,0:T(2,128)}, f32[4,2,2,64,2048]{4,3,2,1,0:T(8,128)}) fusion(f32[4,2,2048,64,2]{2,3,4,1,0:T(8,128)S(1)} %fusion.43, pred[4,64,2048]{2,1,0:T(8,128)(4,1)S(1)} %copy-done.1), kind=kOutput, calls=%fused_computation.68.clone.1 | output fusion | flops 12584959 | bytes 17305600 | tf_op jit(solution)/shard_map/while/body/eval_jaxpr/sub | solution.py:35
  147.8 6.9 %reshape.253 = bf16[4,2048,2,128]{3,2,1,0:T(2,128)(2,1)} reshape(bf16[128,64,256]{2,1,0:T(8,128)(2,1)} %gather_fusion.1) | data formatting | bytes 8388608 | tf_op jit(solution)/shard_map/while/body/eval_jaxpr/reshape | solution.py:108
  154.7 5.9 %fusion.45 = bf16[1,4,64,2,2,128]{5,2,4,3,1,0:T(8,128)(2,1)S(1)} fusion(f32[4,2,2,64,2048]{4,3,2,1,0:T(8,128)} %get-tuple-element.216, f32[4,2,2,64]{3,2,1,0:T(2,128)} %get-tuple-element.217, bf16[4,2048,2,128,1]{3,2,1,0,4:T(2,128)(2,1)} %bitcast.72, pred[4,64]{1,0:T(4,128)(4,1)S(1)} %broadcast_compare_fusion.6), kind=kOutput, calls=%fused_computation.20.clone.1 | convolution fusion | flops 541327360 | bytes 12849408 | tf_op jit(solution)/shard_map/while/body/eval_jaxpr/nkgqp,npkd->nqkgd/dot_general | solution.py:37
  166.0 4.1 %gather_fusion = bf16[128,64,256]{2,1,0:T(8,128)(2,1)} fusion(bf16[40,64,256]{2,1,0:T(8,128)(2,1)} %get-tuple-element.247, s32[1024]{0:T(1024)S(1)} %pad_clamp_fusion.3), kind=kCustom, calls=%fused_computation.1.clone.clone.1 | custom fusion | bytes 8389120 | tf_op jit(solution)/shard_map/while/body/eval_jaxpr/gather | solution.py:107
  170.0 6.9 %reshape.252 = bf16[4,2048,2,128]{3,2,1,0:T(2,128)(2,1)} reshape(bf16[128,64,256]{2,1,0:T(8,128)(2,1)} %gather_fusion) | data formatting | bytes 8388608 | tf_op jit(solution)/shard_map/while/body/eval_jaxpr/reshape | solution.py:107
  181.6 5.9 %fusion.44 = (f32[4,2,2,64]{3,2,1,0:T(2,128)}, f32[4,2,2,64,2048]{4,3,2,1,0:T(8,128)}) fusion(f32[4,2,2048,64,2]{2,3,4,1,0:T(8,128)S(1)} %fusion.43, pred[4,64,2048]{2,1,0:T(8,128)(4,1)S(1)} %copy-done.1), kind=kOutput, calls=%fused_computation.68.clone.1 | output fusion | flops 12584959 | bytes 17305600 | tf_op jit(solution)/shard_map/while/body/eval_jaxpr/sub | solution.py:35
  191.7 6.9 %reshape.253 = bf16[4,2048,2,128]{3,2,1,0:T(2,128)(2,1)} reshape(bf16[128,64,256]{2,1,0:T(8,128)(2,1)} %gather_fusion.1) | data formatting | bytes 8388608 | tf_op jit(solution)/shard_map/while/body/eval_jaxpr/reshape | solution.py:108
  198.6 5.9 %fusion.45 = bf16[1,4,64,2,2,128]{5,2,4,3,1,0:T(8,128)(2,1)S(1)} fusion(f32[4,2,2,64,2048]{4,3,2,1,0:T(8,128)} %get-tuple-element.216, f32[4,2,2,64]{3,2,1,0:T(2,128)} %get-tuple-element.217, bf16[4,2048,2,128,1]{3,2,1,0,4:T(2,128)(2,1)} %bitcast.72, pred[4,64]{1,0:T(4,128)(4,1)S(1)} %broadcast_compare_fusion.6), kind=kOutput, calls=%fused_computation.20.clone.1 | convolution fusion | flops 541327360 | bytes 12849408 | tf_op jit(solution)/shard_map/while/body/eval_jaxpr/nkgqp,npkd->nqkgd/dot_general | solution.py:37
  209.9 4.1 %gather_fusion = bf16[128,64,256]{2,1,0:T(8,128)(2,1)} fusion(bf16[40,64,256]{2,1,0:T(8,128)(2,1)} %get-tuple-element.247, s32[1024]{0:T(1024)S(1)} %pad_clamp_fusion.3), kind=kCustom, calls=%fused_computation.1.clone.clone.1 | custom fusion | bytes 8389120 | tf_op jit(solution)/shard_map/while/body/eval_jaxpr/gather | solution.py:107
  213.9 6.9 %reshape.252 = bf16[4,2048,2,128]{3,2,1,0:T(2,128)(2,1)} reshape(bf16[128,64,256]{2,1,0:T(8,128)(2,1)} %gather_fusion) | data formatting | bytes 8388608 | tf_op jit(solution)/shard_map/while/body/eval_jaxpr/reshape | solution.py:107
  225.5 5.9 %fusion.44 = (f32[4,2,2,64]{3,2,1,0:T(2,128)}, f32[4,2,2,64,2048]{4,3,2,1,0:T(8,128)}) fusion(f32[4,2,2048,64,2]{2,3,4,1,0:T(8,128)S(1)} %fusion.43, pred[4,64,2048]{2,1,0:T(8,128)(4,1)S(1)} %copy-done.1), kind=kOutput, calls=%fused_computation.68.clone.1 | output fusion | flops 12584959 | bytes 17305600 | tf_op jit(solution)/shard_map/while/body/eval_jaxpr/sub | solution.py:35
  235.5 6.9 %reshape.253 = bf16[4,2048,2,128]{3,2,1,0:T(2,128)(2,1)} reshape(bf16[128,64,256]{2,1,0:T(8,128)(2,1)} %gather_fusion.1) | data formatting | bytes 8388608 | tf_op jit(solution)/shard_map/while/body/eval_jaxpr/reshape | solution.py:108
  242.5 5.9 %fusion.45 = bf16[1,4,64,2,2,128]{5,2,4,3,1,0:T(8,128)(2,1)S(1)} fusion(f32[4,2,2,64,2048]{4,3,2,1,0:T(8,128)} %get-tuple-element.216, f32[4,2,2,64]{3,2,1,0:T(2,128)} %get-tuple-element.217, bf16[4,2048,2,128,1]{3,2,1,0,4:T(2,128)(2,1)} %bitcast.72, pred[4,64]{1,0:T(4,128)(4,1)S(1)} %broadcast_compare_fusion.6), kind=kOutput, calls=%fused_computation.20.clone.1 | convolution fusion | flops 541327360 | bytes 12849408 | tf_op jit(solution)/shard_map/while/body/eval_jaxpr/nkgqp,npkd->nqkgd/dot_general | solution.py:37
  250.9 4.3 %convolution_convert_fusion = bf16[1024,2048]{1,0:T(8,128)(2,1)} fusion(bf16[1024,512]{1,0:T(8,128)(2,1)S(1)} %reshape.192, bf16[512,2048]{1,0:T(8,128)(2,1)S(1)} %copy-done), kind=kOutput, calls=%fused_computation.33 | convolution fusion | flops 2149580800 | bytes 7340032 | tf_op jit(solution)/shard_map/dot_general | solution.py:122
  255.2 43.6 %reduce-scatter.2.cloned.1.call-done = bf16[4,256,512]{2,1,0:T(8,128)(2,1)} async-done(((bf16[4,256,2048]{2,1,0:T(8,128)(2,1)}), bf16[4,256,512]{2,1,0:T(8,128)(2,1)}) %reduce-scatter.2.cloned.1.call-update) | async-done | bytes 1048592 | tf_op jit(solution)/shard_map/reduce_scatter | solution.py:130
  (118 shorter events, 71.9 us)
Async XLA Ops:
  6.5 244.3 %copy-start = (bf16[512,2048]{1,0:T(8,128)(2,1)S(1)}, bf16[512,2048]{1,0:T(8,128)(2,1)}, u32[]{:S(2)}) copy-start(bf16[512,2048]{1,0:T(8,128)(2,1)} %param.13) | copy-start | bytes 6291460
  8.9 13.7 %all-to-all-start = ((s32[8,1,3]{2,1,0:T(1,128)}), s32[8,1,3]{2,1,0:T(1,128)S(1)}, u32[]{:S(2)}, u32[]{:S(2)}) async-start(s32[8,1,3]{2,1,0:T(1,128)} %copy.26), calls=%async_computation | async-start | bytes 8192 | tf_op jit(solution)/shard_map/all_to_all | solution.py:82
  19.9 12.4 %copy-start.2 = (bf16[1024,256]{1,0:T(8,128)(2,1)}, bf16[1024,256]{1,0:T(8,128)(2,1)S(1)}, u32[]{:S(2)}) copy-start(bf16[1024,256]{1,0:T(8,128)(2,1)S(1)} %convolution_convert_fusion.3) | copy-start | bytes 1572868
  24.4 23.3 %all-to-all-start.1 = ((bf16[8,3,64,256]{3,2,1,0:T(8,128)(2,1)}), bf16[8,3,64,256]{3,2,1,0:T(8,128)(2,1)}, u32[]{:S(2)}, u32[]{:S(2)}) async-start(bf16[8,3,64,256]{3,2,1,0:T(8,128)(2,1)} %bitcast.4), calls=%async_computation.1 | async-start | bytes 1572864 | tf_op jit(solution)/shard_map/all_to_all | solution.py:85
  32.3 26.0 %copy-start.3 = (bf16[1024,256]{1,0:T(8,128)(2,1)}, bf16[1024,256]{1,0:T(8,128)(2,1)S(1)}, u32[]{:S(2)}) copy-start(bf16[1024,256]{1,0:T(8,128)(2,1)S(1)} %convolution_convert_fusion.2) | copy-start | bytes 1572868
  47.7 23.7 %all-to-all-start.2 = ((bf16[8,3,64,256]{3,2,1,0:T(8,128)(2,1)}), bf16[8,3,64,256]{3,2,1,0:T(8,128)(2,1)}, u32[]{:S(2)}, u32[]{:S(2)}) async-start(bf16[8,3,64,256]{3,2,1,0:T(8,128)(2,1)} %bitcast.78), calls=%async_computation.2 | async-start | bytes 1572864 | tf_op jit(solution)/shard_map/all_to_all | solution.py:84
  51.9 9.4 %copy-start.4 = (s32[4,4,32]{2,1,0:T(4,128)S(1)}, s32[4,4,32]{2,1,0:T(4,128)}, u32[]{:S(2)}) copy-start(s32[4,4,32]{2,1,0:T(4,128)} %param.14) | copy-start | bytes 6148
  51.9 246.8 %reduce-scatter.2.cloned.1.call-start = ((), (), s32[]{:S(2)}) async-start(), calls=%async_computation.4 | async-start | bytes 5242880 | tf_op jit(solution)/shard_map/reduce_scatter | solution.py:130
  63.3 10.5 %copy-start.5 = (s32[4]{0:T(128)S(1)}, s32[4]{0:T(128)}, u32[]{:S(2)}) copy-start(s32[4]{0:T(128)} %add_multiply_fusion) | copy-start | bytes 52
  90.3 3.5 %copy-start.1 = (pred[4,64,2048]{2,1,0:T(8,128)(4,1)S(1)}, pred[4,64,2048]{2,1,0:T(8,128)(4,1)}, u32[]{:S(2)}) copy-start(pred[4,64,2048]{2,1,0:T(8,128)(4,1)} %compare_or_fusion.2) | copy-start | bytes 1572868 | tf_op jit(solution)/shard_map/while
  110.8 6.9 %copy-start.6 = (s32[4]{0:T(128)S(1)}, s32[4]{0:T(128)}, u32[]{:S(2)}) copy-start(s32[4]{0:T(128)} %get-tuple-element.268) | copy-start | bytes 52 | tf_op jit(solution)/shard_map/while
  134.2 3.5 %copy-start.1 = (pred[4,64,2048]{2,1,0:T(8,128)(4,1)S(1)}, pred[4,64,2048]{2,1,0:T(8,128)(4,1)}, u32[]{:S(2)}) copy-start(pred[4,64,2048]{2,1,0:T(8,128)(4,1)} %compare_or_fusion.2) | copy-start | bytes 1572868 | tf_op jit(solution)/shard_map/while
  154.7 6.9 %copy-start.6 = (s32[4]{0:T(128)S(1)}, s32[4]{0:T(128)}, u32[]{:S(2)}) copy-start(s32[4]{0:T(128)} %get-tuple-element.268) | copy-start | bytes 52 | tf_op jit(solution)/shard_map/while
  178.1 3.5 %copy-start.1 = (pred[4,64,2048]{2,1,0:T(8,128)(4,1)S(1)}, pred[4,64,2048]{2,1,0:T(8,128)(4,1)}, u32[]{:S(2)}) copy-start(pred[4,64,2048]{2,1,0:T(8,128)(4,1)} %compare_or_fusion.2) | copy-start | bytes 1572868 | tf_op jit(solution)/shard_map/while
  198.6 6.9 %copy-start.6 = (s32[4]{0:T(128)S(1)}, s32[4]{0:T(128)}, u32[]{:S(2)}) copy-start(s32[4]{0:T(128)} %get-tuple-element.268) | copy-start | bytes 52 | tf_op jit(solution)/shard_map/while
  222.0 3.5 %copy-start.1 = (pred[4,64,2048]{2,1,0:T(8,128)(4,1)S(1)}, pred[4,64,2048]{2,1,0:T(8,128)(4,1)}, u32[]{:S(2)}) copy-start(pred[4,64,2048]{2,1,0:T(8,128)(4,1)} %compare_or_fusion.2) | copy-start | bytes 1572868 | tf_op jit(solution)/shard_map/while
  242.5 6.9 %copy-start.6 = (s32[4]{0:T(128)S(1)}, s32[4]{0:T(128)}, u32[]{:S(2)}) copy-start(s32[4]{0:T(128)} %get-tuple-element.268) | copy-start | bytes 52 | tf_op jit(solution)/shard_map/while
Sparse Core Ops, SparseCore 0:
  255.3 43.3 reduce-scatter.1
where the time goes:
time: 308 us; the launch traced here: 306 us
  local copies, waits for them, and re-layouts  109 us (35%)
  waiting for transfers between devices  66.7 us (22%)
  matrix products  55.6 us (18%)
  other arithmetic  45 us (15%)
  starting transfers between devices  15.9 us (5%)
  between operations  13.5 us (4%)
    reduce_scatter x1, waiting for transfers between devices, shards(): lax.psum_scatter(partial_value.astype(jnp.bfloat16), 'tp', scatter_dimens...  43.6 us
    reshape x4, local copies, waits for them, and re-layouts, one_seq(): value_sets = value_table[seq_rows].reshape(per_dev, TOPK * KB, kv_local, HD)  27.7 us
    reshape x4, local copies, waits for them, and re-layouts, one_seq(): key_sets = key_table[seq_rows].reshape(per_dev, TOPK * KB, kv_local, HD)  27.7 us
    dot_general x4, matrix products, attend(): jnp.einsum('nkgqp,npkd->nqkgd', weights, value_sets, preferred_element_ty...  23.6 us
    sub x4, other arithmetic, attend(): raised = jnp.exp(scores - highest)  23.5 us
    gather x4, local copies, waits for them, and re-layouts, one_seq(): key_sets = key_table[seq_rows].reshape(per_dev, TOPK * KB, kv_local, HD)  16.2 us
    dot_general x4, matrix products, attend(): jnp.einsum('nqkgd,npkd->nkgqp', queries, key_sets, preferred_element_type...  14 us
    all_to_all x1, waiting for transfers between devices, shards(): lax.all_to_all(value_rows[asked], 'kv', split_axis=0, concat_axis=0, tile...  13.8 us
  transfers between devices with their start and end apart: 4, of which 4 were waited for; matrix products, arithmetic and copies ran while one was open for 7% of the time, Pallas kernels for 0%

commit v1 on v0

v1 whole, which is shorter than its diff:
```python
import functools

import jax
import jax.numpy as jnp
from jax import lax
from jax.experimental import pallas as pl
from jax.experimental.pallas import tpu as pltpu
from jax.sharding import PartitionSpec as P

HD = 128
KB = 64
CAP = 3
MASKED = -1e30


def tables(chosen, devices, device):
    batch_size, per_dev, _ = chosen.shape
    blocks = jnp.arange(devices * per_dev, dtype=jnp.int32)
    named = jnp.any(chosen[..., None] == blocks, axis=2)
    named = named.reshape(batch_size, per_dev, devices, per_dev)
    own = jnp.sum(
        jnp.where(jnp.arange(devices)[None, None, :, None] == device, named, False), axis=2
    )
    needed = jnp.any(named, axis=1) & (jnp.arange(devices)[None, :, None] != device)
    needed = jnp.transpose(needed, (1, 0, 2)).reshape(devices, batch_size * per_dev)
    local = jnp.arange(batch_size * per_dev, dtype=jnp.int32)
    slots = jnp.sum(
        jnp.where(local[None, :, None] > local[None, None, :], needed[:, None, :], False),
        axis=2,
        dtype=jnp.int32,
    )
    matches = needed[:, :, None] & (slots[:, :, None] == jnp.arange(CAP, dtype=jnp.int32))
    requests = jnp.sum(jnp.where(matches, local[None, :, None], 0), axis=1)
    matches = matches.reshape(devices, batch_size, per_dev, CAP)
    matches = jnp.transpose(matches, (1, 0, 2, 3))
    remote = jnp.any(named[..., None] & matches[:, None], axis=3)
    own_bias = jnp.where(own > 0, 0.0, MASKED).astype(jnp.float32)
    own_bias = jnp.repeat(own_bias, KB, axis=-1)
    home = device * per_dev + jnp.arange(per_dev, dtype=jnp.int32)
    copies = jnp.sum(chosen == home[None, :, None], axis=-1, dtype=jnp.int32)
    same = jnp.log(jnp.maximum(copies, 1).astype(jnp.float32))
    same = jnp.broadcast_to(same[..., None], own_bias.shape)
    rem_bias = jnp.where(remote, 0.0, MASKED).astype(jnp.float32)
    rem_bias = rem_bias.reshape(batch_size, per_dev, devices // 2, 2 * CAP)
    rem_bias = jnp.repeat(jnp.transpose(rem_bias, (2, 0, 1, 3)), KB, axis=-1)
    return requests, jnp.stack([own_bias, same]), rem_bias


def attend_kernel(
    positions, kv_local, per_group, length_ref, q_ref, k_ref, v_ref, rk_ref, rv_ref,
    own_bias_ref, rem_bias_ref, out_ref, scores_ref
):
    device = lax.axis_index("kv")
    batch_size = own_bias_ref.shape[1]
    per_dev = positions // KB
    wide = rem_bias_ref.shape[-1]
    rows = per_group * positions
    chunks = (device + 1) // 2
    scaling = HD ** (-0.5)
    contract = (((1,), (1,)), ((), ()))

    def masked(scores, bias):
        width = scores.shape[-1]
        shaped = (scores * scaling).reshape(per_group, per_dev, KB, width)
        return (shaped + bias[None, :, None, :]).reshape(rows, width)

    @pl.loop(0, batch_size)
    def _(b):
        live = length_ref[b] - device * positions
        here = pl.ds(pl.multiple_of(b * positions, positions), positions)

        @pl.when(live <= 0)
        def _():
            out_ref[here, :] = jnp.zeros((positions, out_ref.shape[1]), out_ref.dtype)

        @pl.when(live > 0)
        def _():
            at_row = lax.broadcasted_iota(jnp.int32, (positions, positions), 0)
            at_col = lax.broadcasted_iota(jnp.int32, (positions, positions), 1)
            before, same = [
                jnp.broadcast_to(own_bias_ref[i, b][:, None, :], (per_dev, KB, positions)).reshape(
                    positions, positions
                )
                for i in range(2)
            ]
            own_bias = jnp.where(
                at_col < at_row, before, jnp.where(at_col == at_row, same, MASKED)
            )
            living = lax.broadcasted_iota(jnp.int32, (positions, HD), 0) < live
            for h in range(kv_local):
                cols = slice(h * HD, (h + 1) * HD)
                heads = [h * per_group + g for g in range(per_group)]
                queries = jnp.concatenate(
                    [q_ref[here, n * HD:(n + 1) * HD] for n in heads], axis=0
                )
                own = lax.dot_general(
                    queries, k_ref[here, cols], contract, preferred_element_type=jnp.float32
                )
                own = (own * scaling).reshape(per_group, positions, positions) + own_bias[None]
                own = own.reshape(rows, positions)
                top = jnp.max(own, axis=-1, keepdims=True)

                def score(c, top):
                    there = pl.ds(pl.multiple_of(c * wide, wide), wide)
                    far = lax.dot_general(
                        queries, rk_ref[there, cols], contract,
                        preferred_element_type=jnp.float32,
                    )
                    far = masked(far, rem_bias_ref[c, b])
                    scores_ref[c] = far
                    return jnp.maximum(top, jnp.max(far, axis=-1, keepdims=True))

                top = lax.fori_loop(0, chunks, score, top)
                raised = jnp.exp(own - top)
                total = jnp.sum(raised, axis=-1, keepdims=True)
                mixed = jnp.dot(
                    raised.astype(jnp.bfloat16), v_ref[here, cols],
                    preferred_element_type=jnp.float32,
                )

                def gather(c, carry):
                    total, mixed = carry
                    there = pl.ds(pl.multiple_of(c * wide, wide), wide)
                    raised = jnp.exp(scores_ref[c] - top)
                    total = total + jnp.sum(raised, axis=-1, keepdims=True)
                    mixed = mixed + jnp.dot(
                        raised.astype(jnp.bfloat16), rv_ref[there, cols],
                        preferred_element_type=jnp.float32,
                    )
                    return total, mixed

                total, mixed = lax.fori_loop(0, chunks, gather, (total, mixed))
                mixed = mixed / total
                for g, n in enumerate(heads):
                    part = mixed[g * positions:(g + 1) * positions]
                    out_ref[here, n * HD:(n + 1) * HD] = jnp.where(living, part, 0.0).astype(
                        out_ref.dtype
                    )


def attend(positions, kv_local, per_group, lengths, queries, k, v, rk, rv, own_bias, rem_bias):
    vmem = pl.BlockSpec(memory_space=pltpu.VMEM)
    return pl.pallas_call(
        functools.partial(attend_kernel, positions, kv_local, per_group),
        out_shape=jax.ShapeDtypeStruct(queries.shape, jnp.bfloat16),
        in_specs=[pl.BlockSpec(memory_space=pltpu.SMEM)] + [vmem] * 7,
        out_specs=vmem,
        scratch_shapes=[
            pltpu.VMEM(
                (rem_bias.shape[0], per_group * positions, rem_bias.shape[-1]), jnp.float32
            )
        ],
        compiler_params=pltpu.CompilerParams(vmem_limit_bytes=48 * 2**20),
    )(lengths, queries, k, v, rk, rv, own_bias, rem_bias)


def shards(inputs, query_weight, key_weight, value_weight, out_weight, chosen, lengths):
    batch_size, positions, model_width = inputs.shape
    kv_local = key_weight.shape[1] // HD
    heads_local = query_weight.shape[1] // HD
    per_group = heads_local // kv_local
    owned = batch_size * (positions // KB)
    device = lax.axis_index("kv")
    devices = lax.axis_size("kv")
    flat_rows = inputs.reshape(batch_size * positions, model_width)

    def project(weight):
        return jnp.dot(flat_rows, weight, preferred_element_type=jnp.float32).astype(jnp.bfloat16)

    queries = project(query_weight)
    key_rows = project(key_weight)
    value_rows = project(value_weight)
    requests, own_bias, rem_bias = tables(chosen, devices, device)
    asked = lax.all_to_all(requests, "kv", split_axis=0, concat_axis=0, tiled=True)

    def fetch(table):
        picked = table.reshape(owned, KB, kv_local * HD)[asked]
        got = lax.all_to_all(picked, "kv", split_axis=0, concat_axis=0, tiled=True)
        return got.reshape(devices * CAP * KB, kv_local * HD)

    attended = attend(
        positions, kv_local, per_group, lengths, queries, key_rows, value_rows,
        fetch(key_rows), fetch(value_rows), own_bias, rem_bias,
    )
    partial_value = jnp.dot(attended, out_weight, preferred_element_type=jnp.float32).astype(
        jnp.bfloat16
    )
    partial_value = partial_value.reshape(batch_size, positions, model_width)
    return lax.psum_scatter(partial_value, "tp", scatter_dimension=2, tiled=True)


def solution(mesh):
    placed = (
        P(None, "kv", None),
        P(None, "tp"),
        P(None, "tp"),
        P(None, "tp"),
        P("tp", None),
        P(None, "kv", None),
        P(),
    )
    return jax.shard_map(
        shards, mesh=mesh, in_specs=placed, out_specs=P(None, "kv", "tp"), check_vma=False
    )
```

time: 308 us -> 137 us (0.44)
  local copies, waits for them, and re-layouts: 109 us -> 6.68 us
  other arithmetic: 45 us -> 2.03 us
  matrix products: 55.6 us -> 17.9 us
  waiting for transfers between devices: 66.7 us -> 73.6 us
  Pallas kernels: 0 us -> 6.37 us
    reshape x13 -> x3, local copies, waits for them, and re-layouts: 60 us -> 0.38 us  [the longest x2 0.26 us: tables(): named = named.reshape(batch_size, per_dev, devices, per_dev)]
    dot_general x11 -> x3, matrix products: 51.3 us -> 13.7 us  [project(): jnp.dot(flat_rows, weight, preferred_element_type=jnp.float32)]
    gather x10 -> x2, local copies, waits for them, and re-layouts: 30.3 us -> 3.02 us  [fetch(): picked = table.reshape(owned, KB, kv_local * HD)[asked]]
    sub x5 -> x0, other arithmetic: 23.6 us -> none  [the longest x4 23.5 us: attend(): raised = jnp.exp(scores - highest)]
    dynamic_slice x8 -> x0, local copies, waits for them, and re-layouts: 9.59 us -> none  [shards(): lax.map(one_seq, (queries, table_rows, key_pos, unique_key, lengths))]
    lt x8 -> x0, other arithmetic: 8.17 us -> none  [the longest x4 5.55 us: attend(): living = (query_pos < live_length)[:, :, None, None, None]]
    pallas_call x0 -> x1, Pallas kernels: none -> 6.37 us  [attend(): pl.pallas_call(functools.partial(attend_kernel, positions, kv_local, per_...]
    or x4 -> x0, other arithmetic: 6.2 us -> none  [attend(): allowed = allowed | (key_pos[:, None, :] == query_pos[:, :, None])]
  transfers between devices with their start and end apart: 4 -> 4, of which waited for: 4 -> 4; matrix products, arithmetic and copies ran while one was open for 7% -> 12% of each run, Pallas kernels for 0% -> 0%
where the time goes in v1:
time: 137 us; the launch traced here: 136 us
  waiting for transfers between devices  73.6 us (54%)
  matrix products  17.9 us (13%)
  starting transfers between devices  15.7 us (11%)
  between operations  13.6 us (10%)
  local copies, waits for them, and re-layouts  6.68 us (5%)
  Pallas kernels  6.37 us (5%)
  other arithmetic  2.03 us (1%)
    reduce_scatter x1, waiting for transfers between devices, shards(): lax.psum_scatter(partial_value, 'tp', scatter_dimension=2, tiled=True)  45.7 us
    all_to_all x2, waiting for transfers between devices, fetch(): got = lax.all_to_all(picked, 'kv', split_axis=0, concat_axis=0, tiled=True)  25.3 us
    dot_general x3, matrix products, project(): jnp.dot(flat_rows, weight, preferred_element_type=jnp.float32)  13.7 us
    all_to_all x2, starting transfers between devices, fetch(): got = lax.all_to_all(picked, 'kv', split_axis=0, concat_axis=0, tiled=True)  8.41 us
    all_to_all x1, starting transfers between devices, shards(): lax.all_to_all(requests, 'kv', split_axis=0, concat_axis=0, tiled=True)  7.28 us
    pallas_call x1, Pallas kernels, attend(): pl.pallas_call(functools.partial(attend_kernel, positions, kv_local, per_...  6.37 us
    dot_general x1, matrix products, shards(): jnp.dot(attended, out_weight, preferred_element_type=jnp.float32)  4.27 us
    gather x2, local copies, waits for them, and re-layouts, fetch(): picked = table.reshape(owned, KB, kv_local * HD)[asked]  3.02 us
  transfers between devices with their start and end apart: 4, of which 4 were waited for; matrix products, arithmetic and copies ran while one was open for 12% of the time, Pallas kernels for 0%

profile of v1, /device:TPU:0, one launch (start us, length us, event | category | flops | bytes accessed | tf_op | source)
XLA Modules:
  0.0 135.9 jit_solution(6262054121248406408)
XLA Ops:
  6.6 1.0 fusion
  7.6 0.1 reduce_or.30
  7.7 0.1 copy.30
  7.8 0.1 copy.31
  7.9 0.2 convert_reduce_fusion.1
  8.2 0.1 select_reduce_fusion
  8.3 0.7 copy.33
  9.0 7.3 %all-to-all-start = ((s32[8,1,3]{2,1,0:T(1,128)}), s32[8,1,3]{2,1,0:T(1,128)S(1)}, u32[]{:S(2)}, u32[]{:S(2)}) async-start(s32[8,1,3]{2,1,0:T(1,128)} %copy.33), calls=%async_computation | async-start | bytes 8192 | tf_op jit(solution)/shard_map/all_to_all | solution.py:174
  16.3 3.7 %convolution_convert_fusion.3.k_ref = bf16[1024,256]{1,0:T(8,128)(2,1)S(1)} fusion(bf16[1024,2048]{1,0:T(8,128)(2,1)} %bitcast.38, bf16[2048,256]{1,0:T(8,128)(2,1)} %param.9), kind=kOutput, calls=%fused_computation.5 | convolution fusion | flops 1074003968 | bytes 5767168 | tf_op jit(solution)/shard_map/dot_general | solution.py:168
  20.0 2.7 %all-to-all-done = s32[8,1,3]{2,1,0:T(1,128)S(1)} async-done(((s32[8,1,3]{2,1,0:T(1,128)}), s32[8,1,3]{2,1,0:T(1,128)S(1)}, u32[]{:S(2)}, u32[]{:S(2)}) %all-to-all-start) | async-done | bytes 128 | tf_op jit(solution)/shard_map/all_to_all | solution.py:174
  23.0 1.5 %gather_fusion = bf16[24,64,256]{2,1,0:T(8,128)(2,1)} fusion(bf16[16,64,256]{2,1,0:T(8,128)(2,1)S(1)} %bitcast.30, s32[1024]{0:T(1024)S(1)} %pad_clamp_fusion), kind=kCustom, calls=%fused_computation | custom fusion | bytes 1572960 | tf_op jit(solution)/shard_map/gather | solution.py:177
  24.5 4.2 %all-to-all-start.1 = ((bf16[8,3,64,256]{3,2,1,0:T(8,128)(2,1)}), bf16[8,3,64,256]{3,2,1,0:T(8,128)(2,1)}, u32[]{:S(2)}, u32[]{:S(2)}) async-start(bf16[8,3,64,256]{3,2,1,0:T(8,128)(2,1)} %bitcast.6), calls=%async_computation.1 | async-start | bytes 1572864 | tf_op jit(solution)/shard_map/all_to_all | solution.py:178
  28.8 0.1 copy.37
  28.9 0.1 reshape.104
  29.0 0.2 copy.36
  29.2 0.1 convert_reduce_fusion
  29.4 0.1 stack_reshape.3
  29.6 3.7 %convolution_convert_fusion.2.v_ref = bf16[1024,256]{1,0:T(8,128)(2,1)S(1)} fusion(bf16[1024,2048]{1,0:T(8,128)(2,1)} %bitcast.39, bf16[2048,256]{1,0:T(8,128)(2,1)} %param.10), kind=kOutput, calls=%fused_computation.4 | convolution fusion | flops 1074003968 | bytes 5767168 | tf_op jit(solution)/shard_map/dot_general | solution.py:168
  33.4 1.5 %gather_fusion.1 = bf16[24,64,256]{2,1,0:T(8,128)(2,1)} fusion(bf16[16,64,256]{2,1,0:T(8,128)(2,1)S(1)} %bitcast.31, s32[1024]{0:T(1024)S(1)} %pad_clamp_fusion), kind=kCustom, calls=%fused_computation.1 | custom fusion | bytes 1572960 | tf_op jit(solution)/shard_map/gather | solution.py:177
  34.9 12.9 %all-to-all-done.1 = bf16[8,3,64,256]{3,2,1,0:T(8,128)(2,1)} async-done(((bf16[8,3,64,256]{3,2,1,0:T(8,128)(2,1)}), bf16[8,3,64,256]{3,2,1,0:T(8,128)(2,1)}, u32[]{:S(2)}, u32[]{:S(2)}) %all-to-all-start.1) | async-done | bytes 786464 | tf_op jit(solution)/shard_map/all_to_all | solution.py:178
  47.8 4.2 %all-to-all-start.2 = ((bf16[8,3,64,256]{3,2,1,0:T(8,128)(2,1)}), bf16[8,3,64,256]{3,2,1,0:T(8,128)(2,1)}, u32[]{:S(2)}, u32[]{:S(2)}) async-start(bf16[8,3,64,256]{3,2,1,0:T(8,128)(2,1)} %bitcast.33), calls=%async_computation.2 | async-start | bytes 1572864 | tf_op jit(solution)/shard_map/all_to_all | solution.py:178
  52.1 0.2 copy.39
  52.2 0.1 select_n.41
  52.3 0.1 broadcast_in_dim.92
  52.5 0.1 reshape.105.rem_bias_ref
  52.6 0.2 convert_reduce_fusion.2
  52.9 6.2 %convolution_convert_fusion.1.q_ref = bf16[1024,512]{1,0:T(8,128)(2,1)} fusion(bf16[1024,2048]{1,0:T(8,128)(2,1)} %bitcast.40, bf16[2048,512]{1,0:T(8,128)(2,1)} %param.8), kind=kOutput, calls=%fused_computation.3 | convolution fusion | flops 2148007936 | bytes 7340032 | tf_op jit(solution)/shard_map/dot_general | solution.py:168
  59.1 12.4 %all-to-all-done.2 = bf16[8,3,64,256]{3,2,1,0:T(8,128)(2,1)} async-done(((bf16[8,3,64,256]{3,2,1,0:T(8,128)(2,1)}), bf16[8,3,64,256]{3,2,1,0:T(8,128)(2,1)}, u32[]{:S(2)}, u32[]{:S(2)}) %all-to-all-start.2) | async-done | bytes 786464 | tf_op jit(solution)/shard_map/all_to_all | solution.py:178
  71.5 1.2 copy-done.1
  72.7 6.4 %shard_map.73 = bf16[1024,512]{1,0:T(8,128)(2,1)S(1)} custom-call(s32[4]{0:T(128)S(1)} %copy-done.2, bf16[1024,512]{1,0:T(8,128)(2,1)S(1)} %copy-done.1, bf16[1024,256]{1,0:T(8,128)(2,1)S(1)} %convolution_convert_fusion.3.k_ref, bf16[1024,256]{1,0:T(8,128)(2,1)S(1)} %convolution_convert_fusion.2.v_ref, bf16[1536,256]{1,0:T(8,128)(2,1)} %bitcast.7.rk_ref, ...), custom_call_target="tpu_custom_call" | custom-call | tf_op jit(solution)/shard_map/pallas_call | solution.py:143
  79.1 4.3 %convolution_convert_fusion = bf16[1024,2048]{1,0:T(8,128)(2,1)} fusion(bf16[1024,512]{1,0:T(8,128)(2,1)S(1)} %shard_map.73, bf16[512,2048]{1,0:T(8,128)(2,1)S(1)} %copy-done), kind=kOutput, calls=%fused_computation.2 | convolution fusion | flops 2149580800 | bytes 7340032 | tf_op jit(solution)/shard_map/dot_general | solution.py:185
  83.4 45.7 %reduce-scatter.2.cloned.1.call-done = bf16[4,256,512]{2,1,0:T(8,128)(2,1)} async-done(((bf16[4,256,2048]{2,1,0:T(8,128)(2,1)}), bf16[4,256,512]{2,1,0:T(8,128)(2,1)}) %reduce-scatter.2.cloned.1.call-update) | async-done | bytes 1048592 | tf_op jit(solution)/shard_map/reduce_scatter | solution.py:189
  (29 shorter events, 0.9 us)
Async XLA Ops:
  6.5 72.6 %copy-start = (bf16[512,2048]{1,0:T(8,128)(2,1)S(1)}, bf16[512,2048]{1,0:T(8,128)(2,1)}, u32[]{:S(2)}) copy-start(bf16[512,2048]{1,0:T(8,128)(2,1)} %param.11) | copy-start | bytes 6291460
  9.0 13.7 %all-to-all-start = ((s32[8,1,3]{2,1,0:T(1,128)}), s32[8,1,3]{2,1,0:T(1,128)S(1)}, u32[]{:S(2)}, u32[]{:S(2)}) async-start(s32[8,1,3]{2,1,0:T(1,128)} %copy.33), calls=%async_computation | async-start | bytes 8192 | tf_op jit(solution)/shard_map/all_to_all | solution.py:174
  24.5 23.3 %all-to-all-start.1 = ((bf16[8,3,64,256]{3,2,1,0:T(8,128)(2,1)}), bf16[8,3,64,256]{3,2,1,0:T(8,128)(2,1)}, u32[]{:S(2)}, u32[]{:S(2)}) async-start(bf16[8,3,64,256]{3,2,1,0:T(8,128)(2,1)} %bitcast.6), calls=%async_computation.1 | async-start | bytes 1572864 | tf_op jit(solution)/shard_map/all_to_all | solution.py:178
  29.6 23.0 %copy-start.3 = (s32[4,4,32]{2,1,0:T(4,128)S(1)}, s32[4,4,32]{2,1,0:T(4,128)}, u32[]{:S(2)}) copy-start(s32[4,4,32]{2,1,0:T(4,128)} %param.12) | copy-start | bytes 6148
  47.8 23.7 %all-to-all-start.2 = ((bf16[8,3,64,256]{3,2,1,0:T(8,128)(2,1)}), bf16[8,3,64,256]{3,2,1,0:T(8,128)(2,1)}, u32[]{:S(2)}, u32[]{:S(2)}) async-start(bf16[8,3,64,256]{3,2,1,0:T(8,128)(2,1)} %bitcast.33), calls=%async_computation.2 | async-start | bytes 1572864 | tf_op jit(solution)/shard_map/all_to_all | solution.py:178
  52.0 77.1 %reduce-scatter.2.cloned.1.call-start = ((), (), s32[]{:S(2)}) async-start(), calls=%async_computation.4 | async-start | bytes 5242880 | tf_op jit(solution)/shard_map/reduce_scatter | solution.py:189
  52.9 18.6 %copy-start.2 = (s32[4]{0:T(128)S(1)}, s32[4]{0:T(128)}, u32[]{:S(2)}) copy-start(s32[4]{0:T(128)} %length_ref.1) | copy-start | bytes 52
  71.5 1.2 copy-start.1
Sparse Core Ops, SparseCore 0:
  83.5 45.4 reduce-scatter.1

commit v2 on v1

--- a/solution.py
+++ b/solution.py
@@ -154,6 +154,115 @@
     )(lengths, queries, k, v, rk, rv, own_bias, rem_bias)
 
 
+def mix_kernel(
+    steps, tp, att_ref, weight_ref, out_ref,
+    pair_out, pair_in, far_out, far_in, near,
+    pair_sent, pair_got, far_sent, far_got,
+):
+    me = lax.axis_index("tp")
+    core = lax.rem(me, 2)
+    chip = me // 2
+    chips = tp // 2
+    partner = me + 1 - 2 * core
+    width = out_ref.shape[1]
+    step_rows = out_ref.shape[0] // steps
+    mesh_id = pl.DeviceIdType.MESH
+
+    def twin(off):
+        return lax.rem(chip + off, chips) * 2 + core
+
+    barrier = pltpu.get_barrier_semaphore()
+    pl.semaphore_signal(barrier, inc=1, device_id={"tp": partner}, device_id_type=mesh_id)
+    for off in range(1, chips):
+        pl.semaphore_signal(barrier, inc=1, device_id={"tp": twin(off)}, device_id_type=mesh_id)
+    pl.semaphore_wait(barrier, chips)
+
+    def at(i):
+        return pl.ds(pl.multiple_of(i * step_rows, step_rows), step_rows)
+
+    def group_sum(i, off, side):
+        column = (lax.rem(chip + off, chips) * 2 + side) * width
+        return jnp.dot(
+            att_ref[at(i), :],
+            weight_ref[:, pl.ds(pl.multiple_of(column, width), width)],
+            preferred_element_type=jnp.float32,
+        ).astype(jnp.bfloat16)
+
+    def pair_copy(i):
+        return pltpu.make_async_remote_copy(
+            src_ref=pair_out.at[i], dst_ref=pair_in.at[i],
+            send_sem=pair_sent.at[i], recv_sem=pair_got.at[i],
+            device_id={"tp": partner}, device_id_type=mesh_id,
+        )
+
+    def far_copy(i, off):
+        return pltpu.make_async_remote_copy(
+            src_ref=far_out.at[off - 1, i], dst_ref=far_in.at[off - 1, i],
+            send_sem=far_sent.at[off - 1, i], recv_sem=far_got.at[off - 1, i],
+            device_id={"tp": twin(off)}, device_id_type=mesh_id,
+        )
+
+    def step(i, carry):
+        @pl.when(i < steps)
+        def _():
+            for off in range(chips):
+                pair_out[i, off] = group_sum(i, off, 1 - core)
+            pair_copy(i).start()
+
+        @pl.when(i > 0)
+        def _():
+            j = i - 1
+            sums = [group_sum(j, off, core).astype(jnp.float32) for off in range(chips)]
+            pair_copy(j).wait_recv()
+            for off in range(1, chips):
+                both = sums[off] + pair_in[j, off].astype(jnp.float32)
+                far_out[off - 1, j] = both.astype(jnp.bfloat16)
+                far_copy(j, off).start()
+            near[j] = sums[0] + pair_in[j, 0].astype(jnp.float32)
+
+        return carry
+
+    lax.fori_loop(0, steps + 1, step, 0)
+
+    def finish(i, carry):
+        pair_copy(i).wait_send()
+        mixed = near[i]
+        for off in range(1, chips):
+            far_copy(i, off).wait()
+            mixed = mixed + far_in[off - 1, i].astype(jnp.float32)
+        out_ref[at(i), :] = mixed.astype(out_ref.dtype)
+        return carry
+
+    lax.fori_loop(0, steps, finish, 0)
+
+
+def mix(attended, out_weight, tp):
+    rows = attended.shape[0]
+    width = out_weight.shape[1] // tp
+    chips = tp // 2
+    steps = rows // 128
+    vmem = pl.BlockSpec(memory_space=pltpu.VMEM)
+    pair = pltpu.VMEM((steps, chips, rows // steps, width), jnp.bfloat16)
+    far = pltpu.VMEM((chips - 1, steps, rows // steps, width), jnp.bfloat16)
+    return pl.pallas_call(
+        functools.partial(mix_kernel, steps, tp),
+        out_shape=jax.ShapeDtypeStruct((rows, width), jnp.bfloat16),
+        in_specs=[vmem, vmem],
+        out_specs=vmem,
+        scratch_shapes=[
+            pair, pair, far, far,
+            pltpu.VMEM((steps, rows // steps, width), jnp.float32),
+            pltpu.SemaphoreType.DMA((steps,)),
+            pltpu.SemaphoreType.DMA((steps,)),
+            pltpu.SemaphoreType.DMA((chips - 1, steps)),
+            pltpu.SemaphoreType.DMA((chips - 1, steps)),
+        ],
+        compiler_params=pltpu.CompilerParams(
+            collective_id=0, has_side_effects=True, vmem_limit_bytes=48 * 2**20
+        ),
+    )(attended, out_weight)
+
+
 def shards(inputs, query_weight, key_weight, value_weight, out_weight, chosen, lengths):
     batch_size, positions, model_width = inputs.shape
     kv_local = key_weight.shape[1] // HD
@@ -182,11 +291,8 @@
         positions, kv_local, per_group, lengths, queries, key_rows, value_rows,
         fetch(key_rows), fetch(value_rows), own_bias, rem_bias,
     )
-    partial_value = jnp.dot(attended, out_weight, preferred_element_type=jnp.float32).astype(
-        jnp.bfloat16
-    )
-    partial_value = partial_value.reshape(batch_size, positions, model_width)
-    return lax.psum_scatter(partial_value, "tp", scatter_dimension=2, tiled=True)
+    mixed = mix(attended, out_weight, lax.axis_size("tp"))
+    return mixed.reshape(batch_size, positions, -1)
 
 
 def solution(mesh):

time: 137 us -> 103 us (0.75)
  waiting for transfers between devices: 73.6 us -> 28.7 us
  Pallas kernels: 6.37 us -> 34 us
  between operations: 13.6 us -> 0.18 us
  matrix products: 17.9 us -> 13 us
    reduce_scatter x1 -> x0, waiting for transfers between devices: 45.7 us -> none  [shards(): lax.psum_scatter(partial_value, 'tp', scatter_dimension=2, tiled=True)]
    pallas_call x0 -> x1, Pallas kernels: none -> 27.6 us  [mix(): pl.pallas_call(functools.partial(mix_kernel, steps, tp), out_shape=jax.Sh...]
    dot_general x1 -> x0, matrix products: 4.27 us -> none  [shards(): jnp.dot(attended, out_weight, preferred_element_type=jnp.float32)]
  transfers between devices with their start and end apart: 4 -> 3, of which waited for: 4 -> 3; matrix products, arithmetic and copies ran while one was open for 12% -> 16% of each run, Pallas kernels for 0% -> 0%
where the time goes in v2:
time: 103 us; the launch traced here: 101 us
  Pallas kernels  34 us (33%)
  waiting for transfers between devices  28.7 us (28%)
  starting transfers between devices  15.7 us (15%)
  matrix products  13 us (13%)
  local copies, waits for them, and re-layouts  7.81 us (8%)
  other arithmetic  2.03 us (2%)
    pallas_call x1, Pallas kernels, mix(): pl.pallas_call(functools.partial(mix_kernel, steps, tp), out_shape=jax.Sh...  27.6 us
    all_to_all x2, waiting for transfers between devices, fetch(): got = lax.all_to_all(picked, 'kv', split_axis=0, concat_axis=0, tiled=True)  26 us
    dot_general x3, matrix products, project(): jnp.dot(flat_rows, weight, preferred_element_type=jnp.float32)  13 us
    all_to_all x2, starting transfers between devices, fetch(): got = lax.all_to_all(picked, 'kv', split_axis=0, concat_axis=0, tiled=True)  8.41 us
    all_to_all x1, starting transfers between devices, shards(): lax.all_to_all(requests, 'kv', split_axis=0, concat_axis=0, tiled=True)  7.29 us
    pallas_call x1, Pallas kernels, attend(): pl.pallas_call(functools.partial(attend_kernel, positions, kv_local, per_...  6.38 us
    gather x2, local copies, waits for them, and re-layouts, fetch(): picked = table.reshape(owned, KB, kv_local * HD)[asked]  3.02 us
    all_to_all x1, waiting for transfers between devices, shards(): lax.all_to_all(requests, 'kv', split_axis=0, concat_axis=0, tiled=True)  2.68 us
  transfers between devices with their start and end apart: 3, of which 3 were waited for; matrix products, arithmetic and copies ran while one was open for 16% of the time, Pallas kernels for 0%

profile of v2, /device:TPU:0, one launch (start us, length us, event | category | flops | bytes accessed | tf_op | source)
XLA Modules:
  0.0 101.3 jit_solution(5520419952027276414)
XLA Ops:
  0.0 1.0 fusion
  1.0 0.1 reduce_or.30
  1.2 0.1 copy.30
  1.3 0.1 copy.31
  1.4 0.2 convert_reduce_fusion.1
  1.6 0.1 select_reduce_fusion
  1.8 0.7 copy.33
  2.5 7.3 %all-to-all-start = ((s32[8,1,3]{2,1,0:T(1,128)}), s32[8,1,3]{2,1,0:T(1,128)S(1)}, u32[]{:S(2)}, u32[]{:S(2)}) async-start(s32[8,1,3]{2,1,0:T(1,128)} %copy.33), calls=%async_computation | async-start | bytes 8192 | tf_op jit(solution)/shard_map/all_to_all | solution.py:283
  9.7 3.7 %convolution_convert_fusion.2.k_ref = bf16[1024,256]{1,0:T(8,128)(2,1)S(1)} fusion(bf16[1024,2048]{1,0:T(8,128)(2,1)} %bitcast.36, bf16[2048,256]{1,0:T(8,128)(2,1)} %param.9), kind=kOutput, calls=%fused_computation.4 | convolution fusion | flops 1074003968 | bytes 5767168 | tf_op jit(solution)/shard_map/dot_general | solution.py:277
  13.5 2.7 %all-to-all-done = s32[8,1,3]{2,1,0:T(1,128)S(1)} async-done(((s32[8,1,3]{2,1,0:T(1,128)}), s32[8,1,3]{2,1,0:T(1,128)S(1)}, u32[]{:S(2)}, u32[]{:S(2)}) %all-to-all-start) | async-done | bytes 128 | tf_op jit(solution)/shard_map/all_to_all | solution.py:283
  16.4 1.5 %gather_fusion = bf16[24,64,256]{2,1,0:T(8,128)(2,1)} fusion(bf16[16,64,256]{2,1,0:T(8,128)(2,1)S(1)} %bitcast.29, s32[1024]{0:T(1024)S(1)} %pad_clamp_fusion), kind=kCustom, calls=%fused_computation | custom fusion | bytes 1572960 | tf_op jit(solution)/shard_map/gather | solution.py:286
  17.9 4.2 %all-to-all-start.1 = ((bf16[8,3,64,256]{3,2,1,0:T(8,128)(2,1)}), bf16[8,3,64,256]{3,2,1,0:T(8,128)(2,1)}, u32[]{:S(2)}, u32[]{:S(2)}) async-start(bf16[8,3,64,256]{3,2,1,0:T(8,128)(2,1)} %bitcast.6), calls=%async_computation.1 | async-start | bytes 1572864 | tf_op jit(solution)/shard_map/all_to_all | solution.py:287
  22.3 0.1 copy.37
  22.4 0.1 reshape.104
  22.5 0.2 copy.36
  22.7 0.1 convert_reduce_fusion
  22.9 0.1 stack_reshape.3
  23.1 3.7 %convolution_convert_fusion.1.v_ref = bf16[1024,256]{1,0:T(8,128)(2,1)S(1)} fusion(bf16[1024,2048]{1,0:T(8,128)(2,1)} %bitcast.37, bf16[2048,256]{1,0:T(8,128)(2,1)} %param.10), kind=kOutput, calls=%fused_computation.3 | convolution fusion | flops 1074003968 | bytes 5767168 | tf_op jit(solution)/shard_map/dot_general | solution.py:277
  26.8 1.5 %gather_fusion.1 = bf16[24,64,256]{2,1,0:T(8,128)(2,1)} fusion(bf16[16,64,256]{2,1,0:T(8,128)(2,1)S(1)} %bitcast.30, s32[1024]{0:T(1024)S(1)} %pad_clamp_fusion), kind=kCustom, calls=%fused_computation.1 | custom fusion | bytes 1572960 | tf_op jit(solution)/shard_map/gather | solution.py:286
  28.4 12.9 %all-to-all-done.1 = bf16[8,3,64,256]{3,2,1,0:T(8,128)(2,1)} async-done(((bf16[8,3,64,256]{3,2,1,0:T(8,128)(2,1)}), bf16[8,3,64,256]{3,2,1,0:T(8,128)(2,1)}, u32[]{:S(2)}, u32[]{:S(2)}) %all-to-all-start.1) | async-done | bytes 786464 | tf_op jit(solution)/shard_map/all_to_all | solution.py:287
  41.2 4.2 %all-to-all-start.2 = ((bf16[8,3,64,256]{3,2,1,0:T(8,128)(2,1)}), bf16[8,3,64,256]{3,2,1,0:T(8,128)(2,1)}, u32[]{:S(2)}, u32[]{:S(2)}) async-start(bf16[8,3,64,256]{3,2,1,0:T(8,128)(2,1)} %bitcast.31), calls=%async_computation.2 | async-start | bytes 1572864 | tf_op jit(solution)/shard_map/all_to_all | solution.py:287
  45.5 0.2 copy.39
  45.6 0.1 select_n.41
  45.7 0.1 broadcast_in_dim.92
  45.9 0.1 reshape.105.rem_bias_ref
  46.0 0.2 convert_reduce_fusion.2
  46.4 5.5 %convolution_convert_fusion.q_ref = bf16[1024,512]{1,0:T(8,128)(2,1)} fusion(bf16[1024,2048]{1,0:T(8,128)(2,1)} %bitcast.38, bf16[2048,512]{1,0:T(8,128)(2,1)S(1)} %copy-done), kind=kOutput, calls=%fused_computation.2 | convolution fusion | flops 2148007936 | bytes 7340032 | tf_op jit(solution)/shard_map/dot_general | solution.py:277
  51.9 13.1 %all-to-all-done.2 = bf16[8,3,64,256]{3,2,1,0:T(8,128)(2,1)} async-done(((bf16[8,3,64,256]{3,2,1,0:T(8,128)(2,1)}), bf16[8,3,64,256]{3,2,1,0:T(8,128)(2,1)}, u32[]{:S(2)}, u32[]{:S(2)}) %all-to-all-start.2) | async-done | bytes 786464 | tf_op jit(solution)/shard_map/all_to_all | solution.py:287
  65.0 1.4 %copy-done.2 = bf16[1024,512]{1,0:T(8,128)(2,1)S(1)} copy-done((bf16[1024,512]{1,0:T(8,128)(2,1)S(1)}, bf16[1024,512]{1,0:T(8,128)(2,1)}, u32[]{:S(2)}) %copy-start.2) | copy-done | bytes 1048600
  66.3 6.4 %shard_map.73.att_ref = bf16[1024,512]{1,0:T(8,128)(2,1)S(1)} custom-call(s32[4]{0:T(128)S(1)} %copy-done.3, bf16[1024,512]{1,0:T(8,128)(2,1)S(1)} %copy-done.2, bf16[1024,256]{1,0:T(8,128)(2,1)S(1)} %convolution_convert_fusion.2.k_ref, bf16[1024,256]{1,0:T(8,128)(2,1)S(1)} %convolution_convert_fusion.1.v_ref, bf16[1536,256]{1,0:T(8,128)(2,1)} %bitcast.7.rk_ref, ...), custom_call_target="tpu_custom_call" | custom-call | tf_op jit(solution)/shard_map/pallas_call | solution.py:143
  72.7 27.6 %shard_map.74 = bf16[1024,512]{1,0:T(8,128)(2,1)S(1)} custom-call(bf16[1024,512]{1,0:T(8,128)(2,1)S(1)} %shard_map.73.att_ref, bf16[512,2048]{1,0:T(8,128)(2,1)S(1)} %copy-done.1), custom_call_target="tpu_custom_call" | custom-call | tf_op jit(solution)/shard_map/pallas_call | solution.py:247
  100.3 1.0 copy.42
  (29 shorter events, 0.8 us)
Async XLA Ops:
  0.0 46.3 %copy-start = (bf16[2048,512]{1,0:T(8,128)(2,1)S(1)}, bf16[2048,512]{1,0:T(8,128)(2,1)}, u32[]{:S(2)}) copy-start(bf16[2048,512]{1,0:T(8,128)(2,1)} %param.8) | copy-start | bytes 6291460
  2.5 13.7 %all-to-all-start = ((s32[8,1,3]{2,1,0:T(1,128)}), s32[8,1,3]{2,1,0:T(1,128)S(1)}, u32[]{:S(2)}, u32[]{:S(2)}) async-start(s32[8,1,3]{2,1,0:T(1,128)} %copy.33), calls=%async_computation | async-start | bytes 8192 | tf_op jit(solution)/shard_map/all_to_all | solution.py:283
  17.9 23.3 %all-to-all-start.1 = ((bf16[8,3,64,256]{3,2,1,0:T(8,128)(2,1)}), bf16[8,3,64,256]{3,2,1,0:T(8,128)(2,1)}, u32[]{:S(2)}, u32[]{:S(2)}) async-start(bf16[8,3,64,256]{3,2,1,0:T(8,128)(2,1)} %bitcast.6), calls=%async_computation.1 | async-start | bytes 1572864 | tf_op jit(solution)/shard_map/all_to_all | solution.py:287
  23.1 22.9 %copy-start.4 = (s32[4,4,32]{2,1,0:T(4,128)S(1)}, s32[4,4,32]{2,1,0:T(4,128)}, u32[]{:S(2)}) copy-start(s32[4,4,32]{2,1,0:T(4,128)} %param.12) | copy-start | bytes 6148
  41.2 23.7 %all-to-all-start.2 = ((bf16[8,3,64,256]{3,2,1,0:T(8,128)(2,1)}), bf16[8,3,64,256]{3,2,1,0:T(8,128)(2,1)}, u32[]{:S(2)}, u32[]{:S(2)}) async-start(bf16[8,3,64,256]{3,2,1,0:T(8,128)(2,1)} %bitcast.31), calls=%async_computation.2 | async-start | bytes 1572864 | tf_op jit(solution)/shard_map/all_to_all | solution.py:287
  46.4 18.6 %copy-start.3 = (s32[4]{0:T(128)S(1)}, s32[4]{0:T(128)}, u32[]{:S(2)}) copy-start(s32[4]{0:T(128)} %length_ref.1) | copy-start | bytes 52
  65.0 7.8 %copy-start.1 = (bf16[512,2048]{1,0:T(8,128)(2,1)S(1)}, bf16[512,2048]{1,0:T(8,128)(2,1)}, u32[]{:S(2)}) copy-start(bf16[512,2048]{1,0:T(8,128)(2,1)} %weight_ref.1) | copy-start | bytes 6291460
  65.0 1.4 %copy-start.2 = (bf16[1024,512]{1,0:T(8,128)(2,1)S(1)}, bf16[1024,512]{1,0:T(8,128)(2,1)}, u32[]{:S(2)}) copy-start(bf16[1024,512]{1,0:T(8,128)(2,1)} %convolution_convert_fusion.q_ref) | copy-start | bytes 3145732

commit v3 on v2

--- a/solution.py
+++ b/solution.py
@@ -47,7 +47,7 @@
 
 
 def attend_kernel(
-    positions, kv_local, per_group, length_ref, q_ref, k_ref, v_ref, rk_ref, rv_ref,
+    positions, kv_local, per_group, length_ref, q_ref, k_ref, v_ref, rem_ref,
     own_bias_ref, rem_bias_ref, out_ref, scores_ref
 ):
     device = lax.axis_index("kv")
@@ -89,6 +89,7 @@
             living = lax.broadcasted_iota(jnp.int32, (positions, HD), 0) < live
             for h in range(kv_local):
                 cols = slice(h * HD, (h + 1) * HD)
+                far_cols = slice((kv_local + h) * HD, (kv_local + h + 1) * HD)
                 heads = [h * per_group + g for g in range(per_group)]
                 queries = jnp.concatenate(
                     [q_ref[here, n * HD:(n + 1) * HD] for n in heads], axis=0
@@ -103,7 +104,7 @@
                 def score(c, top):
                     there = pl.ds(pl.multiple_of(c * wide, wide), wide)
                     far = lax.dot_general(
-                        queries, rk_ref[there, cols], contract,
+                        queries, rem_ref[there, cols], contract,
                         preferred_element_type=jnp.float32,
                     )
                     far = masked(far, rem_bias_ref[c, b])
@@ -124,7 +125,7 @@
                     raised = jnp.exp(scores_ref[c] - top)
                     total = total + jnp.sum(raised, axis=-1, keepdims=True)
                     mixed = mixed + jnp.dot(
-                        raised.astype(jnp.bfloat16), rv_ref[there, cols],
+                        raised.astype(jnp.bfloat16), rem_ref[there, far_cols],
                         preferred_element_type=jnp.float32,
                     )
                     return total, mixed
@@ -138,12 +139,12 @@
                     )
 
 
-def attend(positions, kv_local, per_group, lengths, queries, k, v, rk, rv, own_bias, rem_bias):
+def attend(positions, kv_local, per_group, lengths, queries, k, v, rem, own_bias, rem_bias):
     vmem = pl.BlockSpec(memory_space=pltpu.VMEM)
     return pl.pallas_call(
         functools.partial(attend_kernel, positions, kv_local, per_group),
         out_shape=jax.ShapeDtypeStruct(queries.shape, jnp.bfloat16),
-        in_specs=[pl.BlockSpec(memory_space=pltpu.SMEM)] + [vmem] * 7,
+        in_specs=[pl.BlockSpec(memory_space=pltpu.SMEM)] + [vmem] * 6,
         out_specs=vmem,
         scratch_shapes=[
             pltpu.VMEM(
@@ -151,7 +152,7 @@
             )
         ],
         compiler_params=pltpu.CompilerParams(vmem_limit_bytes=48 * 2**20),
-    )(lengths, queries, k, v, rk, rv, own_bias, rem_bias)
+    )(lengths, queries, k, v, rem, own_bias, rem_bias)
 
 
 def mix_kernel(
@@ -282,14 +283,18 @@
     requests, own_bias, rem_bias = tables(chosen, devices, device)
     asked = lax.all_to_all(requests, "kv", split_axis=0, concat_axis=0, tiled=True)
 
-    def fetch(table):
-        picked = table.reshape(owned, KB, kv_local * HD)[asked]
-        got = lax.all_to_all(picked, "kv", split_axis=0, concat_axis=0, tiled=True)
-        return got.reshape(devices * CAP * KB, kv_local * HD)
-
+    picked = jnp.concatenate(
+        [
+            table.reshape(owned, KB, kv_local * HD)[asked]
+            for table in (key_rows, value_rows)
+        ],
+        axis=-1,
+    )
+    got = lax.all_to_all(picked, "kv", split_axis=0, concat_axis=0, tiled=True)
+    got = got.reshape(devices * CAP * KB, 2 * kv_local * HD)
     attended = attend(
         positions, kv_local, per_group, lengths, queries, key_rows, value_rows,
-        fetch(key_rows), fetch(value_rows), own_bias, rem_bias,
+        got, own_bias, rem_bias,
     )
     mixed = mix(attended, out_weight, lax.axis_size("tp"))
     return mixed.reshape(batch_size, positions, -1)

time: 103 us -> 101 us (0.981)
  starting transfers between devices: 15.7 us -> 12.2 us
  other arithmetic: 2.03 us -> 4.71 us
  matrix products: 13 us -> 10.6 us
  waiting for transfers between devices: 28.7 us -> 30.3 us
    all_to_all x2 -> x1, starting transfers between devices: 8.41 us -> 4.9 us  [shards(): got = lax.all_to_all(picked, 'kv', split_axis=0, concat_axis=0, tiled=True)]
    all_to_all x2 -> x1, waiting for transfers between devices: 26 us -> 29.2 us  [shards(): got = lax.all_to_all(picked, 'kv', split_axis=0, concat_axis=0, tiled=True)]
    concatenate x0 -> x1, other arithmetic: none -> 2.68 us  [shards(): jnp.concatenate([table.reshape(owned, KB, kv_local * HD)[asked] for table...]
    dot_general x3, matrix products: 13 us -> 10.6 us  [project(): jnp.dot(flat_rows, weight, preferred_element_type=jnp.float32)]
    all_to_all x1, waiting for transfers between devices: 2.68 us -> 1.11 us  [shards(): lax.all_to_all(requests, 'kv', split_axis=0, concat_axis=0, tiled=True)]
    unnamed x11 -> x15, local copies, waits for them, and re-layouts: 2.37 us -> 2.51 us
  transfers between devices with their start and end apart: 3 -> 2, of which waited for: 3 -> 2; matrix products, arithmetic and copies ran while one was open for 16% -> 12% of each run, Pallas kernels for 0% -> 0%
where the time goes in v3:
time: 101 us; the launch traced here: 100 us
  Pallas kernels  34 us (34%)
  waiting for transfers between devices  30.3 us (30%)
  starting transfers between devices  12.2 us (12%)
  matrix products  10.6 us (10%)
  local copies, waits for them, and re-layouts  7.94 us (8%)
  other arithmetic  4.71 us (5%)
    all_to_all x1, waiting for transfers between devices, shards(): got = lax.all_to_all(picked, 'kv', split_axis=0, concat_axis=0, tiled=True)  29.2 us
    pallas_call x1, Pallas kernels, mix(): pl.pallas_call(functools.partial(mix_kernel, steps, tp), out_shape=jax.Sh...  27.6 us
    dot_general x3, matrix products, project(): jnp.dot(flat_rows, weight, preferred_element_type=jnp.float32)  10.6 us
    all_to_all x1, starting transfers between devices, shards(): lax.all_to_all(requests, 'kv', split_axis=0, concat_axis=0, tiled=True)  7.29 us
    pallas_call x1, Pallas kernels, attend(): pl.pallas_call(functools.partial(attend_kernel, positions, kv_local, per_...  6.41 us
    all_to_all x1, starting transfers between devices, shards(): got = lax.all_to_all(picked, 'kv', split_axis=0, concat_axis=0, tiled=True)  4.9 us
    gather x2, local copies, waits for them, and re-layouts, shards(): table.reshape(owned, KB, kv_local * HD)[asked]  3.02 us
    concatenate x1, other arithmetic, shards(): jnp.concatenate([table.reshape(owned, KB, kv_local * HD)[asked] for table...  2.68 us
  transfers between devices with their start and end apart: 2, of which 2 were waited for; matrix products, arithmetic and copies ran while one was open for 12% of the time, Pallas kernels for 0%

profile of v3, /device:TPU:0, one launch (start us, length us, event | category | flops | bytes accessed | tf_op | source)
XLA Modules:
  0.0 100.0 jit_solution(1616549767664905131)
XLA Ops:
  0.0 1.0 %fusion = (pred[4,4,32]{2,1,0:T(4,128)(4,1)S(1)}, pred[4,32]{1,0:T(4,128)(4,1)S(1)}) fusion(s32[4,4,32]{2,1,0:T(4,128)} %param.12), kind=kLoop, calls=%fused_computation.7 | loop fusion | flops 48512 | bytes 2688 | tf_op jit(solution)/shard_map/reduce_or | solution.py:19
  1.0 0.1 reduce_or.30
  1.2 0.1 copy.30
  1.3 0.1 copy.31
  1.4 0.2 convert_reduce_fusion.1
  1.6 0.1 select_reduce_fusion
  1.8 0.7 copy.33
  2.5 7.3 %all-to-all-start = ((s32[8,1,3]{2,1,0:T(1,128)}), s32[8,1,3]{2,1,0:T(1,128)S(1)}, u32[]{:S(2)}, u32[]{:S(2)}) async-start(s32[8,1,3]{2,1,0:T(1,128)} %copy.33), calls=%async_computation | async-start | bytes 8192 | tf_op jit(solution)/shard_map/all_to_all | solution.py:284
  9.8 3.9 %convolution_convert_fusion.1.v_ref = bf16[1024,256]{1,0:T(8,128)(2,1)S(1)} fusion(bf16[1024,2048]{1,0:T(8,128)(2,1)} %bitcast.36, bf16[2048,256]{1,0:T(8,128)(2,1)} %param.10), kind=kOutput, calls=%fused_computation.4 | convolution fusion | flops 1074003968 | bytes 5767168 | tf_op jit(solution)/shard_map/dot_general | solution.py:278
  13.7 0.1 copy-done.6
  13.8 1.2 %convolution_convert_fusion.2.k_ref = bf16[1024,256]{1,0:T(8,128)(2,1)S(1)} fusion(bf16[1024,2048]{1,0:T(8,128)(2,1)S(1)} %bitcast.38, bf16[2048,256]{1,0:T(8,128)(2,1)S(1)} %copy-done.6), kind=kOutput, calls=%fused_computation.5 | convolution fusion | flops 1074003968 | bytes 5767168 | tf_op jit(solution)/shard_map/dot_general | solution.py:278
  15.1 1.1 %all-to-all-done = s32[8,1,3]{2,1,0:T(1,128)S(1)} async-done(((s32[8,1,3]{2,1,0:T(1,128)}), s32[8,1,3]{2,1,0:T(1,128)S(1)}, u32[]{:S(2)}, u32[]{:S(2)}) %all-to-all-start) | async-done | bytes 128 | tf_op jit(solution)/shard_map/all_to_all | solution.py:284
  16.4 1.5 %gather_fusion = bf16[24,64,256]{2,1,0:T(8,128)(2,1)} fusion(bf16[16,64,256]{2,1,0:T(8,128)(2,1)S(1)} %bitcast.29, s32[1024]{0:T(1024)S(1)} %pad_clamp_fusion), kind=kCustom, calls=%fused_computation | custom fusion | bytes 1572960 | tf_op jit(solution)/shard_map/gather | solution.py:288
  17.9 1.5 %gather_fusion.1 = bf16[24,64,256]{2,1,0:T(8,128)(2,1)} fusion(bf16[16,64,256]{2,1,0:T(8,128)(2,1)S(1)} %bitcast.28, s32[1024]{0:T(1024)S(1)} %pad_clamp_fusion), kind=kCustom, calls=%fused_computation.1 | custom fusion | bytes 1572960 | tf_op jit(solution)/shard_map/gather | solution.py:288
  19.4 2.7 %pad_maximum_fusion = bf16[8,3,64,512]{3,2,1,0:T(8,128)(2,1)} fusion(bf16[8,3,64,256]{3,2,1,0:T(8,128)(2,1)} %bitcast.31, bf16[8,3,64,256]{3,2,1,0:T(8,128)(2,1)} %bitcast.30), kind=kLoop, calls=%fused_computation.2 | loop fusion | flops 3145728 | bytes 3145728 | tf_op jit(solution)/shard_map/concatenate | solution.py:286
  22.1 4.9 %all-to-all-start.1 = ((bf16[8,3,64,512]{3,2,1,0:T(8,128)(2,1)}), bf16[8,3,64,512]{3,2,1,0:T(8,128)(2,1)}, u32[]{:S(2)}, u32[]{:S(2)}) async-start(bf16[8,3,64,512]{3,2,1,0:T(8,128)(2,1)} %pad_maximum_fusion), calls=%async_computation.1 | async-start | bytes 3145728 | tf_op jit(solution)/shard_map/all_to_all | solution.py:293
  27.2 0.1 copy.37
  27.3 0.1 reshape.100
  27.4 0.2 copy.36
  27.6 0.1 convert_reduce_fusion
  27.8 0.1 stack_reshape.3
  28.0 0.2 copy.39
  28.2 0.1 select_n.41
  28.3 0.1 broadcast_in_dim.92
  28.4 0.1 reshape.101.rem_bias_ref
  28.5 0.2 convert_reduce_fusion.2
  28.9 5.5 %convolution_convert_fusion.q_ref = bf16[1024,512]{1,0:T(8,128)(2,1)} fusion(bf16[1024,2048]{1,0:T(8,128)(2,1)} %bitcast.37, bf16[2048,512]{1,0:T(8,128)(2,1)S(1)} %copy-done), kind=kOutput, calls=%fused_computation.3 | convolution fusion | flops 2148007936 | bytes 7340032 | tf_op jit(solution)/shard_map/dot_general | solution.py:278
  34.4 29.2 %all-to-all-done.1 = bf16[8,3,64,512]{3,2,1,0:T(8,128)(2,1)} async-done(((bf16[8,3,64,512]{3,2,1,0:T(8,128)(2,1)}), bf16[8,3,64,512]{3,2,1,0:T(8,128)(2,1)}, u32[]{:S(2)}, u32[]{:S(2)}) %all-to-all-start.1) | async-done | bytes 1572896 | tf_op jit(solution)/shard_map/all_to_all | solution.py:293
  63.6 1.4 %copy-done.2 = bf16[1024,512]{1,0:T(8,128)(2,1)S(1)} copy-done((bf16[1024,512]{1,0:T(8,128)(2,1)S(1)}, bf16[1024,512]{1,0:T(8,128)(2,1)}, u32[]{:S(2)}) %copy-start.2) | copy-done | bytes 1048600
  65.0 6.4 %shard_map.73.att_ref = bf16[1024,512]{1,0:T(8,128)(2,1)S(1)} custom-call(s32[4]{0:T(128)S(1)} %copy-done.3, bf16[1024,512]{1,0:T(8,128)(2,1)S(1)} %copy-done.2, bf16[1024,256]{1,0:T(8,128)(2,1)S(1)} %convolution_convert_fusion.2.k_ref, bf16[1024,256]{1,0:T(8,128)(2,1)S(1)} %convolution_convert_fusion.1.v_ref, bf16[1536,512]{1,0:T(8,128)(2,1)} %bitcast.9.rem_ref, ...), custom_call_target="tpu_custom_call" | custom-call | tf_op jit(solution)/shard_map/pallas_call | solution.py:144
  71.4 27.6 %shard_map.74 = bf16[1024,512]{1,0:T(8,128)(2,1)S(1)} custom-call(bf16[1024,512]{1,0:T(8,128)(2,1)S(1)} %shard_map.73.att_ref, bf16[512,2048]{1,0:T(8,128)(2,1)S(1)} %copy-done.1), custom_call_target="tpu_custom_call" | custom-call | tf_op jit(solution)/shard_map/pallas_call | solution.py:248
  99.0 1.0 copy.42
  (32 shorter events, 0.8 us)
Async XLA Ops:
  0.0 28.9 %copy-start = (bf16[2048,512]{1,0:T(8,128)(2,1)S(1)}, bf16[2048,512]{1,0:T(8,128)(2,1)}, u32[]{:S(2)}) copy-start(bf16[2048,512]{1,0:T(8,128)(2,1)} %param.8) | copy-start | bytes 6291460
  2.5 13.7 %all-to-all-start = ((s32[8,1,3]{2,1,0:T(1,128)}), s32[8,1,3]{2,1,0:T(1,128)S(1)}, u32[]{:S(2)}, u32[]{:S(2)}) async-start(s32[8,1,3]{2,1,0:T(1,128)} %copy.33), calls=%async_computation | async-start | bytes 8192 | tf_op jit(solution)/shard_map/all_to_all | solution.py:284
  9.7 3.9 %copy-start.5 = (bf16[4,256,2048]{2,1,0:T(8,128)(2,1)S(1)}, bf16[4,256,2048]{2,1,0:T(8,128)(2,1)}, u32[]{:S(2)}) copy-start(bf16[4,256,2048]{2,1,0:T(8,128)(2,1)} %param.7) | copy-start | bytes 12582916
  9.8 4.1 %copy-start.6 = (bf16[2048,256]{1,0:T(8,128)(2,1)S(1)}, bf16[2048,256]{1,0:T(8,128)(2,1)}, u32[]{:S(2)}) copy-start(bf16[2048,256]{1,0:T(8,128)(2,1)} %param.9) | copy-start | bytes 3145732
  19.4 9.1 %copy-start.4 = (s32[4,4,32]{2,1,0:T(4,128)S(1)}, s32[4,4,32]{2,1,0:T(4,128)}, u32[]{:S(2)}) copy-start(s32[4,4,32]{2,1,0:T(4,128)} %param.12) | copy-start | bytes 6148
  22.1 41.4 %all-to-all-start.1 = ((bf16[8,3,64,512]{3,2,1,0:T(8,128)(2,1)}), bf16[8,3,64,512]{3,2,1,0:T(8,128)(2,1)}, u32[]{:S(2)}, u32[]{:S(2)}) async-start(bf16[8,3,64,512]{3,2,1,0:T(8,128)(2,1)} %pad_maximum_fusion), calls=%async_computation.1 | async-start | bytes 3145728 | tf_op jit(solution)/shard_map/all_to_all | solution.py:293
  28.9 34.7 %copy-start.3 = (s32[4]{0:T(128)S(1)}, s32[4]{0:T(128)}, u32[]{:S(2)}) copy-start(s32[4]{0:T(128)} %length_ref.1) | copy-start | bytes 52
  63.6 7.8 %copy-start.1 = (bf16[512,2048]{1,0:T(8,128)(2,1)S(1)}, bf16[512,2048]{1,0:T(8,128)(2,1)}, u32[]{:S(2)}) copy-start(bf16[512,2048]{1,0:T(8,128)(2,1)} %weight_ref.1) | copy-start | bytes 6291460
  63.6 1.4 %copy-start.2 = (bf16[1024,512]{1,0:T(8,128)(2,1)S(1)}, bf16[1024,512]{1,0:T(8,128)(2,1)}, u32[]{:S(2)}) copy-start(bf16[1024,512]{1,0:T(8,128)(2,1)} %convolution_convert_fusion.q_ref) | copy-start | bytes 3145732
